TPU v7x, 32 devices: a whole 2x2x4 slice. The times are simulated.
32 devices in a mesh: fs: 8 (over z, y), tp: 4 (over x, core).
Axes of the slice: x: 2, y: 2, z: 4, core: 2. Of those that a mesh axis runs over, the one named last changes fastest.
Arguments:
- block_input: bfloat16 [1536, 2048], P('fs'), may hold values from -6 to 6
- query_cotangent: bfloat16 [1536, 1024], P('fs', 'tp'), may hold values from -0.15625 to 0.15625
- key_cotangent: bfloat16 [1536, 1024], P('fs', 'tp'), may hold values from -0.15625 to 0.15625
- query_factor: bfloat16 [2048, 256], P('fs'), may hold values from -0.125 to 0.125
- key_factor: bfloat16 [2048, 256], P('fs'), may hold values from -0.125 to 0.125
- query_first: float32 [256, 1024], P('fs', 'tp'), may hold values from -0.6 to 0.6
- query_second: float32 [256, 1024], P('fs', 'tp'), may hold values from 0.005 to 0.03
- key_first: float32 [256, 1024], P('fs', 'tp'), may hold values from -0.6 to 0.6
- key_second: float32 [256, 1024], P('fs', 'tp'), may hold values from 0.005 to 0.03
- query_weight: float32 [2048, 1024], P('fs', 'tp'), may hold values from -0.125 to 0.125
- key_weight: float32 [2048, 1024], P('fs', 'tp'), may hold values from -0.125 to 0.125
Outputs:
- query_update: float32 [2048, 1024], P('fs', 'tp')
- query_new: float32 [2048, 1024], P('fs', 'tp')
- query_copy: bfloat16 [2048, 1024], P(None, 'tp')
- query_first_new: float32 [256, 1024], P('fs', 'tp')
- query_second_new: float32 [256, 1024], P('fs', 'tp')
- key_update: float32 [2048, 1024], P('fs', 'tp')
- key_new: float32 [2048, 1024], P('fs', 'tp')
- key_copy: bfloat16 [2048, 1024], P(None, 'tp')
- key_first_new: float32 [256, 1024], P('fs', 'tp')
- key_second_new: float32 [256, 1024], P('fs', 'tp')
All inputs are finite; a program needn't handle non-finite values.
Results may differ from a plain program's by a relative error of at most 0.0005.
Values may be sent and summed in bfloat16 or wider, within the bound.
A program may use at most 64 MiB of HBM per device.

v0:
```python
import jax
import jax.numpy as jnp
from jax import lax
from jax.sharding import PartitionSpec as P

beta_one = 0.9
beta_two = 0.99
denom_floor = 0.001
scale_floor = 0.5
learn_rate = 0.02


def moments(small, first, second):
    first_new = beta_one * first + (1.0 - beta_one) * small
    second_new = beta_two * second + (1.0 - beta_two) * small * small
    direction = first_new / (jnp.sqrt(second_new) + denom_floor)
    return (first_new, second_new, direction)


def split_three(values):
    upper = lax.optimization_barrier(values.astype(jnp.bfloat16))
    rest = values - upper.astype(jnp.float32)
    middle = lax.optimization_barrier(rest.astype(jnp.bfloat16))
    lower = (rest - middle.astype(jnp.float32)).astype(jnp.bfloat16)
    return (upper, middle, lower)


def project_tokens(mixed, cotangent):
    contract = (((0,), (0,)), ((), ()))
    total = jnp.zeros((mixed.shape[1], cotangent.shape[1]), jnp.float32)
    for piece in split_three(mixed):
        total = total + lax.dot_general(
            piece, cotangent, contract, preferred_element_type=jnp.float32
        )
    return total


def body(
    block_input,
    query_cotangent,
    key_cotangent,
    query_factor,
    key_factor,
    query_first,
    query_second,
    key_first,
    key_second,
    query_weight,
    key_weight,
):
    query_wide = query_factor.astype(jnp.float32)
    key_wide = key_factor.astype(jnp.float32)
    whole_query, whole_key = (
        lax.all_gather(query_factor, "fs", axis=0, tiled=True),
        lax.all_gather(key_factor, "fs", axis=0, tiled=True),
    )
    mixed_query = jnp.dot(block_input, whole_query, preferred_element_type=jnp.float32)
    mixed_key = jnp.dot(block_input, whole_key, preferred_element_type=jnp.float32)
    query_part = project_tokens(mixed_query, query_cotangent)
    key_part = project_tokens(mixed_key, key_cotangent)
    small_query, small_key = (
        lax.psum_scatter(query_part, "fs", scatter_dimension=0, tiled=True),
        lax.psum_scatter(key_part, "fs", scatter_dimension=0, tiled=True),
    )
    query_first_new, query_second_new, query_direction = moments(
        small_query, query_first, query_second
    )
    key_first_new, key_second_new, key_direction = moments(small_key, key_first, key_second)
    full_query, full_key = (
        lax.all_gather(query_direction, "fs", axis=0, tiled=True),
        lax.all_gather(key_direction, "fs", axis=0, tiled=True),
    )
    query_square, key_square = lax.psum(
        (jnp.sum(query_direction * query_direction), jnp.sum(key_direction * key_direction)),
        ("fs", "tp"),
    )
    entry_count = full_query.shape[0] * full_query.shape[1] * lax.axis_size("tp")
    query_scale = 1.0 / jnp.maximum(jnp.sqrt(query_square / entry_count), scale_floor)
    key_scale = 1.0 / jnp.maximum(jnp.sqrt(key_square / entry_count), scale_floor)
    query_update = -query_scale * jnp.dot(query_wide, full_query, precision=lax.Precision.HIGHEST)
    key_update = -key_scale * jnp.dot(key_wide, full_key, precision=lax.Precision.HIGHEST)
    query_new = query_weight + learn_rate * query_update
    key_new = key_weight + learn_rate * key_update
    query_copy, key_copy = (
        lax.all_gather(query_new.astype(jnp.bfloat16), "fs", axis=0, tiled=True),
        lax.all_gather(key_new.astype(jnp.bfloat16), "fs", axis=0, tiled=True),
    )
    return (
        query_update,
        query_new,
        query_copy,
        query_first_new,
        query_second_new,
        key_update,
        key_new,
        key_copy,
        key_first_new,
        key_second_new,
    )


def solution(mesh):
    in_specs = (
        P("fs", None),
        P("fs", "tp"),
        P("fs", "tp"),
        P("fs", None),
        P("fs", None),
        P("fs", "tp"),
        P("fs", "tp"),
        P("fs", "tp"),
        P("fs", "tp"),
        P("fs", "tp"),
        P("fs", "tp"),
    )
    out_specs = (
        P("fs", "tp"),
        P("fs", "tp"),
        P(None, "tp"),
        P("fs", "tp"),
        P("fs", "tp"),
        P("fs", "tp"),
        P("fs", "tp"),
        P(None, "tp"),
        P("fs", "tp"),
        P("fs", "tp"),
    )
    return jax.shard_map(body, mesh=mesh, in_specs=in_specs, out_specs=out_specs, check_vma=False)
```

profile of v0, /device:TPU:0, one launch (start us, length us, event | category | flops | bytes accessed | tf_op | source)
XLA Modules:
  0.0 387.7 jit_solution(9742643711055467736)
XLA Ops:
  7.2 0.0 copy-start
  7.2 0.0 all-gather.5.cloned.1.call-start
  7.2 0.7 all-gather.5.cloned.1.call-update
  7.9 0.0 all-gather.9.cloned.1.call-start
  8.0 0.7 all-gather.9.cloned.1.call-update
  8.7 0.0 reduce-scatter.5.cloned.1.call-start
  8.7 44.4 %all-gather.5.cloned.1.call-done = bf16[2048,256]{1,0:T(8,128)(2,1)} async-done(((bf16[256,256]{1,0:T(8,128)(2,1)}), bf16[2048,256]{1,0:T(8,128)(2,1)}) %all-gather.5.cloned.1.call-update) | async-done | bytes 1048592 | tf_op jit(solution)/shard_map/all_gather | solution.py:54
  53.2 1.6 fusion.10
  54.8 39.5 %all-gather.9.cloned.1.call-done = bf16[2048,256]{1,0:T(8,128)(2,1)} async-done(((bf16[256,256]{1,0:T(8,128)(2,1)}), bf16[2048,256]{1,0:T(8,128)(2,1)}) %all-gather.9.cloned.1.call-update) | async-done | bytes 1048592 | tf_op jit(solution)/shard_map/all_gather | solution.py:55
  94.3 1.6 fusion.11
  95.9 0.0 copy-start.1
  96.0 0.9 copy-done.1
  96.8 0.2 fusion.13
  97.0 0.2 convolution_add_fusion.1
  97.3 0.9 convolution_add_fusion
  98.2 0.0 reduce-scatter.5.cloned.1.call-update
  98.2 0.0 reduce-scatter.3.cloned.1.call-start
  98.3 0.8 copy-done.2
  99.1 0.2 fusion.12
  99.3 0.2 convolution_add_fusion.3
  99.6 0.9 convolution_add_fusion.2
  100.5 0.0 reduce-scatter.3.cloned.1.call-update
  100.6 0.0 copy-start.8
  100.6 0.0 all-gather.7.cloned.1.call-start
  100.6 0.8 copy-done.5
  101.5 0.1 copy.21
  101.6 0.0 copy-start.9
  101.6 57.5 %reduce-scatter.5.cloned.1.call-done = f32[32,256]{1,0:T(8,128)} async-done(((f32[256,256]{1,0:T(8,128)}), f32[32,256]{1,0:T(8,128)}) %reduce-scatter.5.cloned.1.call-update) | async-done | bytes 32784 | tf_op jit(solution)/shard_map/reduce_scatter | solution.py:63
  159.1 2.0 multiply_reduce_fusion
  161.1 62.9 %reduce-scatter.3.cloned.1.call-done = f32[32,256]{1,0:T(8,128)} async-done(((f32[256,256]{1,0:T(8,128)}), f32[32,256]{1,0:T(8,128)}) %reduce-scatter.3.cloned.1.call-update) | async-done | bytes 32784 | tf_op jit(solution)/shard_map/reduce_scatter | solution.py:62
  224.0 2.0 multiply_reduce_fusion.1
  226.0 40.4 %all-reduce = (f32[]{:T(128)}, f32[]{:T(128)}) all-reduce(f32[]{:T(128)} %get-tuple-element.30, f32[]{:T(128)} %get-tuple-element.26), channel_id=1, replica_groups=mesh['fs'=8,'tp'=4] {'fs','tp'}, use_global_device_ids=true, to_apply=%region_2.0 | all-reduce | flops 2 | bytes 16 | tf_op jit(solution)/shard_map/psum | solution.py:73
  267.2 30.9 %all_gather.19 = f32[256,256]{1,0:T(8,128)S(1)} all-gather(f32[32,256]{1,0:T(8,128)S(1)} %get-tuple-element.31), channel_id=1, replica_groups=mesh['fs'=8,'tp'=4] {'fs'}, dimensions={0}, use_global_device_ids=true | all-gather | bytes 294912 | tf_op jit(solution)/shard_map/all_gather | solution.py:70
  298.0 1.0 fusion.7
  299.1 0.0 all-gather.7.cloned.1.call-update
  299.1 0.0 all-gather.11.cloned.1.call-start
  299.2 0.1 copy.22
  300.1 31.5 %all_gather.22 = f32[256,256]{1,0:T(8,128)S(1)} all-gather(f32[32,256]{1,0:T(8,128)S(1)} %get-tuple-element.27), channel_id=1, replica_groups=mesh['fs'=8,'tp'=4] {'fs'}, dimensions={0}, use_global_device_ids=true | all-gather | bytes 294912 | tf_op jit(solution)/shard_map/all_gather | solution.py:71
  331.6 1.0 fusion.6
  332.6 0.0 all-gather.11.cloned.1.call-update
  332.6 0.8 copy.24
  333.5 0.8 copy.23
  334.3 0.8 copy.27
  335.1 0.8 copy.26
  336.0 2.5 all-gather.7.cloned.1.call-done
  338.5 2.3 copy.25
  340.8 37.9 %all-gather.11.cloned.1.call-done = bf16[2048,256]{0,1:T(8,128)(2,1)} async-done(((bf16[256,256]{0,1:T(8,128)(2,1)}), bf16[2048,256]{0,1:T(8,128)(2,1)}) %all-gather.11.cloned.1.call-update) | async-done | bytes 1048592 | tf_op jit(solution)/shard_map/all_gather | solution.py:86
  378.6 2.3 copy.28
  (17 shorter events, 0.1 us)
Async XLA Ops:
  7.2 46.0 %copy-start = (bf16[192,2048]{1,0:T(8,128)(2,1)S(1)}, bf16[192,2048]{1,0:T(8,128)(2,1)}, u32[]{:S(2)}) copy-start(bf16[192,2048]{1,0:T(8,128)(2,1)} %param.11) | copy-start | bytes 2359300
  7.2 46.0 %all-gather.5.cloned.1.call-start = ((), (), s32[]{:S(2)}) async-start(), calls=%async_computation.2 | async-start | bytes 1179648 | tf_op jit(solution)/shard_map/all_gather | solution.py:54
  7.9 86.4 %all-gather.9.cloned.1.call-start = ((), (), s32[]{:S(2)}) async-start(), calls=%async_computation.5 | async-start | bytes 1179648 | tf_op jit(solution)/shard_map/all_gather | solution.py:55
  8.7 150.4 %reduce-scatter.5.cloned.1.call-start = ((), (), s32[]{:S(2)}) async-start(), calls=%async_computation.6 | async-start | bytes 294912 | tf_op jit(solution)/shard_map/reduce_scatter | solution.py:63
  95.9 0.9 copy-start.1
  98.2 0.9 copy-start.2
  98.2 125.8 %reduce-scatter.3.cloned.1.call-start = ((), (), s32[]{:S(2)}) async-start(), calls=%async_computation.3 | async-start | bytes 294912 | tf_op jit(solution)/shard_map/reduce_scatter | solution.py:62
  100.5 0.9 copy-start.5
  100.6 58.5 %copy-start.7 = (f32[32,256]{1,0:T(8,128)S(1)}, f32[32,256]{1,0:T(8,128)}, u32[]{:S(2)}) copy-start(f32[32,256]{1,0:T(8,128)} %param.19) | copy-start | bytes 98308
  100.6 58.5 %copy-start.8 = (f32[32,256]{1,0:T(8,128)S(1)}, f32[32,256]{1,0:T(8,128)}, u32[]{:S(2)}) copy-start(f32[32,256]{1,0:T(8,128)} %param.18) | copy-start | bytes 98308
  100.6 237.9 %all-gather.7.cloned.1.call-start = ((), (), s32[]{:S(2)}) async-start(), calls=%async_computation.4 | async-start | bytes 1179648 | tf_op jit(solution)/shard_map/all_gather | solution.py:85
  101.6 122.4 %copy-start.9 = (f32[32,256]{1,0:T(8,128)S(1)}, f32[32,256]{1,0:T(8,128)}, u32[]{:S(2)}) copy-start(f32[32,256]{1,0:T(8,128)} %param.17) | copy-start | bytes 98308
  101.6 122.4 %copy-start.10 = (f32[32,256]{1,0:T(8,128)S(1)}, f32[32,256]{1,0:T(8,128)}, u32[]{:S(2)}) copy-start(f32[32,256]{1,0:T(8,128)} %param.16) | copy-start | bytes 98308
  267.2 30.9 %copy-start.3 = (bf16[256,256]{1,0:T(8,128)(2,1)S(1)}, bf16[256,256]{1,0:T(8,128)(2,1)}, u32[]{:S(2)}) copy-start(bf16[256,256]{1,0:T(8,128)(2,1)} %param.14) | copy-start | bytes 393220
  298.0 1.1 copy-start.6
  299.1 79.5 %all-gather.11.cloned.1.call-start = ((), (), s32[]{:S(2)}) async-start(), calls=%async_computation.7 | async-start | bytes 1179648 | tf_op jit(solution)/shard_map/all_gather | solution.py:86
  300.0 31.5 %copy-start.4 = (bf16[256,256]{1,0:T(8,128)(2,1)S(1)}, bf16[256,256]{1,0:T(8,128)(2,1)}, u32[]{:S(2)}) copy-start(bf16[256,256]{1,0:T(8,128)(2,1)} %param.15) | copy-start | bytes 393220
Sparse Core Ops, SparseCore 0:
  10.1 42.9 all-gather.4
  55.3 38.9 all-gather.8
  98.3 60.6 reduce-scatter.4
  162.8 61.1 reduce-scatter.2
  299.2 39.2 all-gather.6
  340.4 38.1 all-gather.10
where the time goes:
time: 388 us
  waiting for transfers between devices  246 us (63%)
  blocking collectives  103 us (27%)
  between operations  15.7 us (4%)
  local copies, waits for them, and re-layouts  10.7 us (3%)
  matrix products  8.06 us (2%)
  other arithmetic  4.02 us (1%)
    reduce_scatter x1, waiting for transfers between devices, body(): lax.psum_scatter(query_part, 'fs', scatter_dimension=0, tiled=True)  62.9 us
    reduce_scatter x1, waiting for transfers between devices, body(): lax.psum_scatter(key_part, 'fs', scatter_dimension=0, tiled=True)  57.5 us
    all_gather x1, waiting for transfers between devices, body(): lax.all_gather(query_factor, 'fs', axis=0, tiled=True)  44.4 us
    psum x1, blocking collectives, body(): lax.psum((jnp.sum(query_direction * query_direction), jnp.sum(key_directi...  40.4 us
    all_gather x1, waiting for transfers between devices, body(): lax.all_gather(key_factor, 'fs', axis=0, tiled=True)  39.5 us
    all_gather x1, waiting for transfers between devices, body(): lax.all_gather(key_new.astype(jnp.bfloat16), 'fs', axis=0, tiled=True)  37.9 us
    all_gather x1, blocking collectives, body(): lax.all_gather(key_direction, 'fs', axis=0, tiled=True)  31.5 us
    all_gather x1, blocking collectives, body(): lax.all_gather(query_direction, 'fs', axis=0, tiled=True)  30.9 us
  transfers between devices with their start and end apart: 6, of which 6 were waited for; matrix products, arithmetic and copies ran while one was open for 3% of the time, Pallas kernels for 0%

commit v1 on v0

--- a/solution.py
+++ b/solution.py
@@ -1,6 +1,10 @@
+import functools
+
 import jax
 import jax.numpy as jnp
 from jax import lax
+from jax.experimental import pallas as pl
+from jax.experimental.pallas import tpu as pltpu
 from jax.sharding import PartitionSpec as P
 
 beta_one = 0.9
@@ -8,6 +12,8 @@
 denom_floor = 0.001
 scale_floor = 0.5
 learn_rate = 0.02
+MESH = pl.DeviceIdType.MESH
+ANY = pl.BlockSpec(memory_space=pl.ANY)
 
 
 def moments(small, first, second):
@@ -15,6 +21,397 @@
     second_new = beta_two * second + (1.0 - beta_two) * small * small
     direction = first_new / (jnp.sqrt(second_new) + denom_floor)
     return (first_new, second_new, direction)
+
+
+def split_two(values):
+    upper = values.astype(jnp.bfloat16)
+    lower = (values - upper.astype(jnp.float32)).astype(jnp.bfloat16)
+    return (upper, lower)
+
+
+def ring_place(index, n):
+    odd = index % 2
+    along = index // 2
+    return (1 - odd) * along + odd * (n - 1 - along)
+
+
+def ring_index(place, n):
+    back = place // (n // 2)
+    return (1 - back) * (2 * place) + back * (2 * (n - 1 - place) + 1)
+
+
+class Ring:
+    def __init__(self, n, me, own, slot, send, recv):
+        self.n, self.own, self.slot, self.send, self.recv = n, own, slot, send, recv
+        self.me = me
+        self.place = ring_place(me, n)
+        self.last = n // 2
+
+    def active(self, step, way, half):
+        return step < self.last or (step == self.last and way == half)
+
+    def owner(self, step, way):
+        shift = -step if way == 0 else step
+        return ring_index((self.place + shift + self.n) % self.n, self.n)
+
+    def copy(self, step, way, half):
+        shift = 1 if way == 0 else self.n - 1
+        to = ring_index((self.place + shift) % self.n, self.n)
+        if step == 1:
+            owner, src = self.me, self.own(half)
+        else:
+            owner = self.owner(step - 1, way)
+            src = self.slot(owner, half)
+        return pltpu.make_async_remote_copy(
+            src_ref=src,
+            dst_ref=self.slot(owner, half),
+            send_sem=self.send.at[way, step - 1, half],
+            recv_sem=self.recv.at[way, step - 1, half],
+            device_id={"fs": to},
+            device_id_type=MESH,
+        )
+
+    def begin(self, half):
+        for way in range(2):
+            if self.active(1, way, half):
+                self.copy(1, way, half).start()
+
+    def step(self, step, arrived):
+        for half in range(2):
+            for way in range(2):
+                if self.active(step, way, half):
+                    self.copy(step, way, half).wait_recv()
+                    if self.active(step + 1, way, half):
+                        self.copy(step + 1, way, half).start()
+                    arrived(self.owner(step, way), half)
+
+    def finish(self):
+        for step in range(1, self.last + 1):
+            for way in range(2):
+                for half in range(2):
+                    if self.active(step, way, half):
+                        self.copy(step, way, half).wait_send()
+
+
+def fused(
+    n,
+    tps,
+    x_in,
+    cq_in,
+    ck_in,
+    fq_in,
+    fk_in,
+    q1_in,
+    q2_in,
+    k1_in,
+    k2_in,
+    wq_in,
+    wk_in,
+    uq_out,
+    nq_out,
+    cq_out,
+    q1_out,
+    q2_out,
+    uk_out,
+    nk_out,
+    ck_out,
+    k1_out,
+    k2_out,
+    x,
+    cot,
+    fac,
+    first,
+    second,
+    weight,
+    gathered,
+    mix,
+    part,
+    landed,
+    dirs,
+    squares,
+    update,
+    fresh,
+    copies,
+    in_sem,
+    out_sem,
+    copy_sem,
+    ring_a_send,
+    ring_a_recv,
+    ring_e_send,
+    ring_e_recv,
+    mix_send,
+    mix_recv,
+    part_send,
+    part_recv,
+    dir_send,
+    dir_recv,
+    sq_send,
+    sq_recv,
+):
+    me = lax.axis_index("fs")
+    tp = lax.axis_index("tp")
+    core = tp % 2
+    rows = fac.shape[1]
+    half_rows = rows // 2
+    rank_rows = first.shape[1]
+    rank = n * rank_rows
+    width = cot.shape[2]
+
+    loads = [
+        pltpu.make_async_copy(src, dst, in_sem.at[i])
+        for i, (src, dst) in enumerate(
+            (
+                (fq_in, fac.at[0]),
+                (fk_in, fac.at[1]),
+                (x_in, x),
+                (cq_in, cot.at[0]),
+                (ck_in, cot.at[1]),
+                (q1_in, first.at[0]),
+                (k1_in, first.at[1]),
+                (q2_in, second.at[0]),
+                (k2_in, second.at[1]),
+                (wq_in, weight.at[0]),
+                (wk_in, weight.at[1]),
+            )
+        )
+    ]
+    for load in loads:
+        load.start()
+
+    barrier = pltpu.get_barrier_semaphore()
+    for k in range(1, n):
+        pl.semaphore_signal(barrier, inc=1, device_id={"fs": (me + k) % n}, device_id_type=MESH)
+    for k in range(1, tps):
+        pl.semaphore_signal(barrier, inc=1, device_id={"tp": (tp + k) % tps}, device_id_type=MESH)
+    pl.semaphore_wait(barrier, n + tps - 2)
+
+    loads[0].wait()
+    loads[1].wait()
+    ring = Ring(
+        n,
+        me,
+        lambda half: fac.at[core, pl.ds(half * half_rows, half_rows)],
+        lambda owner, half: gathered.at[owner, pl.ds(half * half_rows, half_rows)],
+        ring_a_send,
+        ring_a_recv,
+    )
+    ring.begin(0)
+    ring.begin(1)
+    loads[2].wait()
+
+    def product(owner, low, size, block):
+        columns = pl.ds(pl.multiple_of(owner * rows + low, 128), size)
+        mix[core] += jnp.dot(x[:, columns], block, preferred_element_type=jnp.float32)
+
+    mix[core] = jnp.dot(
+        x[:, pl.ds(pl.multiple_of(me * rows, 128), rows)],
+        fac[core],
+        preferred_element_type=jnp.float32,
+    )
+    for step in range(1, n // 2 + 1):
+        seen = []
+        ring.step(step, lambda owner, half: seen.append((owner, half)))
+        if step < n // 2:
+            for way in range(2):
+                owner = ring.owner(step, way)
+                product(owner, 0, rows, gathered[owner])
+        else:
+            product(ring.owner(step, 0), 0, rows, gathered[ring.owner(step, 0)])
+
+    swap = pltpu.make_async_remote_copy(
+        src_ref=mix.at[core],
+        dst_ref=mix.at[core],
+        send_sem=mix_send,
+        recv_sem=mix_recv,
+        device_id={"tp": tp + 1 - 2 * core},
+        device_id_type=MESH,
+    )
+    swap.start()
+    ring.finish()
+    for load in loads[3:]:
+        load.wait()
+    swap.wait()
+
+    contract = (((0,), (0,)), ((), ()))
+    for p in range(2):
+        upper, lower = split_two(mix[p])
+        total = lax.dot_general(upper, cot[p], contract, preferred_element_type=jnp.float32)
+        total += lax.dot_general(lower, cot[p], contract, preferred_element_type=jnp.float32)
+        part[:, p] = total.reshape(n, rank_rows, width)
+
+    def share(k):
+        to = (me + k) % n
+        return pltpu.make_async_remote_copy(
+            src_ref=part.at[to],
+            dst_ref=landed.at[me],
+            send_sem=part_send.at[k - 1],
+            recv_sem=part_recv.at[k - 1],
+            device_id={"fs": to},
+            device_id_type=MESH,
+        )
+
+    for k in range(1, n):
+        share(k).start()
+    small = part[me]
+    for k in range(1, n):
+        share(k).wait_recv()
+        small += landed[(me - k + n) % n]
+
+    first_new, second_new, direction = moments(small, first[...], second[...])
+    dirs[me] = direction
+
+    def spread(k):
+        return pltpu.make_async_remote_copy(
+            src_ref=dirs.at[me],
+            dst_ref=dirs.at[me],
+            send_sem=dir_send.at[k - 1],
+            recv_sem=dir_recv.at[k - 1],
+            device_id={"fs": (me + k) % n},
+            device_id_type=MESH,
+        )
+
+    for k in range(1, n):
+        spread(k).start()
+    first[...] = first_new
+    second[...] = second_new
+    outs = [
+        pltpu.make_async_copy(src, dst, out_sem.at[i])
+        for i, (src, dst) in enumerate(
+            (
+                (first.at[0], q1_out),
+                (first.at[1], k1_out),
+                (second.at[0], q2_out),
+                (second.at[1], k2_out),
+                (update.at[0], uq_out),
+                (update.at[1], uk_out),
+                (fresh.at[0], nq_out),
+                (fresh.at[1], nk_out),
+            )
+        )
+    ]
+    for out in outs[:4]:
+        out.start()
+    for k in range(1, n):
+        share(k).wait_send()
+    for k in range(1, n):
+        spread(k).wait_recv()
+
+    full = [dirs[:, p].reshape(rank, width) for p in range(2)]
+    for p in range(2):
+        squares[tp, p] = jnp.sum((full[p] * full[p]).reshape(rank // 8, 8, width), axis=0)
+
+    def tell(k):
+        return pltpu.make_async_remote_copy(
+            src_ref=squares.at[tp],
+            dst_ref=squares.at[tp],
+            send_sem=sq_send.at[k - 1],
+            recv_sem=sq_recv.at[k - 1],
+            device_id={"tp": (tp + k) % tps},
+            device_id_type=MESH,
+        )
+
+    for k in range(1, tps):
+        tell(k).start()
+    for p in range(2):
+        upper, lower = split_two(full[p])
+        total = jnp.dot(fac[p], upper, preferred_element_type=jnp.float32)
+        update[p] = total + jnp.dot(fac[p], lower, preferred_element_type=jnp.float32)
+    for k in range(1, tps):
+        tell(k).wait_recv()
+
+    ring = Ring(
+        n,
+        me,
+        lambda half: copies.at[me, half],
+        lambda owner, half: copies.at[owner, half],
+        ring_e_send,
+        ring_e_recv,
+    )
+    targets = (cq_out, ck_out)
+
+    def put(owner, half):
+        return pltpu.make_async_copy(
+            copies.at[owner, half],
+            targets[half].at[pl.ds(pl.multiple_of(owner * rows, 16), rows)],
+            copy_sem.at[owner, half],
+        )
+
+    for p in range(2):
+        square = jnp.sum(jnp.sum(squares[:, p], axis=0), keepdims=True)
+        scale = 1.0 / jnp.maximum(jnp.sqrt(square / (rank * width * tps)), scale_floor)
+        step = -scale * update[p]
+        made = weight[p] + learn_rate * step
+        copies[me, p] = made.astype(jnp.bfloat16)
+        ring.begin(p)
+        update[p] = step
+        fresh[p] = made
+        put(me, p).start()
+        outs[4 + p].start()
+        outs[6 + p].start()
+
+    for step in range(1, n // 2 + 1):
+        ring.step(step, lambda owner, half: put(owner, half).start())
+    for k in range(1, n):
+        spread(k).wait_send()
+    for k in range(1, tps):
+        tell(k).wait_send()
+    ring.finish()
+    for out in outs:
+        out.wait()
+    for owner in range(n):
+        for half in range(2):
+            put(owner, half).wait()
+
+
+def fused_body(n, tps, *args):
+    x, cot, _, fac, _, first, _, _, _, weight, _ = args
+    bf16, f32 = jnp.bfloat16, jnp.float32
+    rows, rank = fac.shape
+    width = cot.shape[1]
+    rank_rows = first.shape[0]
+    matrix = jax.ShapeDtypeStruct((rows, width), f32)
+    copy = jax.ShapeDtypeStruct((rows * n, width), bf16)
+    moment = jax.ShapeDtypeStruct((rank_rows, width), f32)
+    dma = pltpu.SemaphoreType.DMA
+    return pl.pallas_call(
+        functools.partial(fused, n, tps),
+        out_shape=(matrix, matrix, copy, moment, moment) * 2,
+        in_specs=[ANY] * 11,
+        out_specs=(ANY,) * 10,
+        scratch_shapes=[
+            pltpu.VMEM(x.shape, bf16),
+            pltpu.VMEM((2,) + cot.shape, bf16),
+            pltpu.VMEM((2,) + fac.shape, bf16),
+            pltpu.VMEM((2,) + first.shape, f32),
+            pltpu.VMEM((2,) + first.shape, f32),
+            pltpu.VMEM((2, rows, width), f32),
+            pltpu.VMEM((n,) + fac.shape, bf16),
+            pltpu.VMEM((2, x.shape[0], rank), f32),
+            pltpu.VMEM((n, 2) + first.shape, f32),
+            pltpu.VMEM((n, 2) + first.shape, f32),
+            pltpu.VMEM((n, 2) + first.shape, f32),
+            pltpu.VMEM((tps, 2, 8, width), f32),
+            pltpu.VMEM((2, rows, width), f32),
+            pltpu.VMEM((2, rows, width), f32),
+            pltpu.VMEM((n, 2, rows, width), bf16),
+            dma((11,)),
+            dma((8,)),
+            dma((n, 2)),
+            dma((2, n // 2, 2)),
+            dma((2, n // 2, 2)),
+            dma((2, n // 2, 2)),
+            dma((2, n // 2, 2)),
+            dma,
+            dma,
+            dma((n - 1,)),
+            dma((n - 1,)),
+            dma((n - 1,)),
+            dma((n - 1,)),
+            dma((tps - 1,)),
+            dma((tps - 1,)),
+        ],
+        compiler_params=pltpu.CompilerParams(collective_id=0, has_side_effects=True),
+    )(*args)
 
 
 def split_three(values):
@@ -35,7 +432,7 @@
     return total
 
 
-def body(
+def plain_body(
     block_input,
     query_cotangent,
     key_cotangent,
@@ -100,29 +497,16 @@
 
 
 def solution(mesh):
-    in_specs = (
-        P("fs", None),
-        P("fs", "tp"),
-        P("fs", "tp"),
-        P("fs", None),
-        P("fs", None),
-        P("fs", "tp"),
-        P("fs", "tp"),
-        P("fs", "tp"),
-        P("fs", "tp"),
-        P("fs", "tp"),
-        P("fs", "tp"),
-    )
-    out_specs = (
-        P("fs", "tp"),
-        P("fs", "tp"),
-        P(None, "tp"),
-        P("fs", "tp"),
-        P("fs", "tp"),
-        P("fs", "tp"),
-        P("fs", "tp"),
-        P(None, "tp"),
-        P("fs", "tp"),
-        P("fs", "tp"),
-    )
+    n, tps = mesh.shape["fs"], mesh.shape["tp"]
+    split = P("fs", "tp")
+    in_specs = (P("fs", None), split, split, P("fs", None), P("fs", None)) + (split,) * 6
+    out_specs = (split, split, P(None, "tp"), split, split) * 2
+
+    def body(*args):
+        factor, first = args[3], args[5]
+        whole_tiles = first.shape[0] % 8 == 0 and factor.shape[0] % 128 == 0
+        if n % 2 == 0 and tps % 2 == 0 and whole_tiles:
+            return fused_body(n, tps, *args)
+        return plain_body(*args)
+
     return jax.shard_map(body, mesh=mesh, in_specs=in_specs, out_specs=out_specs, check_vma=False)

time: 388 us -> 88.1 us (0.23)
  waiting for transfers between devices: 246 us -> 0 us
  blocking collectives: 103 us -> 0 us
  Pallas kernels: 0 us -> 77.7 us
  between operations: 15.7 us -> 0.69 us
  matrix products: 8.06 us -> 0 us
  other arithmetic: 4.02 us -> 0 us
    all_gather x4 -> x0, waiting for transfers between devices: 124 us -> none  [the longest x1 44.4 us: body(): lax.all_gather(query_factor, 'fs', axis=0, tiled=True)]
    reduce_scatter x2 -> x0, waiting for transfers between devices: 120 us -> none  [the longest x1 62.9 us: body(): lax.psum_scatter(query_part, 'fs', scatter_dimension=0, tiled=True)]
    pallas_call x0 -> x1, Pallas kernels: none -> 77.7 us  [fused_body(): pl.pallas_call(functools.partial(fused, n, tps), out_shape=(matrix, matri...]
    all_gather x2 -> x0, blocking collectives: 62.4 us -> none  [the longest x1 31.5 us: body(): lax.all_gather(key_direction, 'fs', axis=0, tiled=True)]
    psum x1 -> x0, blocking collectives: 40.4 us -> none  [body(): lax.psum((jnp.sum(query_direction * query_direction), jnp.sum(key_directi...]
    dot_general x10 -> x0, matrix products: 8.06 us -> none  [the longest x6 2.77 us: project_tokens(): lax.dot_general(piece, cotangent, contract, preferred_element_type=jnp.fl...]
    reduce_sum x2 -> x0, other arithmetic: 3.98 us -> none  [the longest x1 1.99 us: body(): jnp.sum(key_direction * key_direction)]
    unnamed x30 -> x26, local copies, waits for them, and re-layouts: 10.7 us -> 9.41 us
  transfers between devices with their start and end apart: 6 -> 0, of which waited for: 6 -> 0; matrix products, arithmetic and copies ran while one was open for 3% -> 0% of each run, Pallas kernels for 0% -> 0%
where the time goes in v1:
time: 88.1 us; the launch traced here: 87.8 us
  Pallas kernels  77.7 us (88%)
  local copies, waits for them, and re-layouts  9.41 us (11%)
    pallas_call x1, Pallas kernels, fused_body(): pl.pallas_call(functools.partial(fused, n, tps), out_shape=(matrix, matri...  77.7 us
    unnamed x26, local copies, waits for them, and re-layouts  9.41 us

profile of v1, /device:TPU:0, one launch (start us, length us, event | category | flops | bytes accessed | tf_op | source)
XLA Modules:
  0.0 87.8 jit_solution(11004841779808251248)
XLA Ops:
  0.6 77.7 %shard_map.186 = (f32[256,256]{1,0:T(8,128)}, f32[256,256]{1,0:T(8,128)}, bf16[2048,256]{1,0:T(8,128)(2,1)}, f32[32,256]{1,0:T(8,128)}, f32[32,256]{1,0:T(8,128)...) custom-call(bf16[192,2048]{1,0:T(8,128)(2,1)} %x_in.1, ...), custom_call_target="tpu_custom_call" | custom-call | tf_op jit(solution)/shard_map/pallas_call | solution.py:376
  78.4 0.0 copy-start.1
  78.4 1.8 %copy.31 = f32[256,256]{1,0:T(8,128)} copy(f32[256,256]{1,0:T(8,128)} %get-tuple-element.20) | data formatting | bytes 524288
  80.2 1.7 %copy.32 = f32[256,256]{1,0:T(8,128)} copy(f32[256,256]{1,0:T(8,128)} %get-tuple-element.21) | data formatting | bytes 524288
  81.8 0.0 copy-done.1
  81.8 0.0 copy-start.7
  81.8 0.0 copy-start.6
  81.8 0.0 copy-start.3
  81.8 0.0 copy-start.2
  81.9 1.0 %copy.33 = bf16[2048,256]{1,0:T(8,128)(2,1)} copy(bf16[2048,256]{1,0:T(8,128)(2,1)S(1)} %copy-done.1) | data formatting | bytes 2097152
  82.8 0.0 copy-done.7
  82.8 0.0 copy-start
  82.8 0.6 copy.34
  83.4 0.0 copy-done.6
  83.5 0.6 copy.35
  84.1 0.0 copy-done.3
  84.1 0.7 copy.36
  84.8 0.0 copy-done.2
  84.8 0.7 copy.37
  85.5 0.0 copy-done
  85.5 0.0 copy-start.5
  85.5 1.0 %copy.38 = bf16[2048,256]{1,0:T(8,128)(2,1)} copy(bf16[2048,256]{1,0:T(8,128)(2,1)S(1)} %copy-done) | data formatting | bytes 2097152
  86.5 0.0 copy-done.5
  86.5 0.0 copy-start.4
  86.5 0.6 copy.39
  87.1 0.2 copy-done.4
  87.2 0.6 copy.40
Async XLA Ops:
  78.4 3.4 %copy-start.1 = (bf16[2048,256]{1,0:T(8,128)(2,1)S(1)}, bf16[2048,256]{1,0:T(8,128)(2,1)}, u32[]{:S(2)}) copy-start(bf16[2048,256]{1,0:T(8,128)(2,1)} %get-tuple-element.22) | copy-start | bytes 3145732
  81.8 1.0 %copy-start.7 = (f32[32,256]{1,0:T(8,128)S(1)}, f32[32,256]{1,0:T(8,128)}, u32[]{:S(2)}) copy-start(f32[32,256]{1,0:T(8,128)} %get-tuple-element.23) | copy-start | bytes 98308
  81.8 1.6 %copy-start.6 = (f32[32,256]{1,0:T(8,128)S(1)}, f32[32,256]{1,0:T(8,128)}, u32[]{:S(2)}) copy-start(f32[32,256]{1,0:T(8,128)} %get-tuple-element.24) | copy-start | bytes 98308
  81.8 2.2 %copy-start.3 = (f32[256,256]{1,0:T(8,128)S(1)}, f32[256,256]{1,0:T(8,128)}, u32[]{:S(2)}) copy-start(f32[256,256]{1,0:T(8,128)} %get-tuple-element.25) | copy-start | bytes 786436
  81.8 2.9 %copy-start.2 = (f32[256,256]{1,0:T(8,128)S(1)}, f32[256,256]{1,0:T(8,128)}, u32[]{:S(2)}) copy-start(f32[256,256]{1,0:T(8,128)} %get-tuple-element.26) | copy-start | bytes 786436
  82.8 2.6 %copy-start = (bf16[2048,256]{1,0:T(8,128)(2,1)S(1)}, bf16[2048,256]{1,0:T(8,128)(2,1)}, u32[]{:S(2)}) copy-start(bf16[2048,256]{1,0:T(8,128)(2,1)} %get-tuple-element.27) | copy-start | bytes 3145732
  85.5 1.0 %copy-start.5 = (f32[32,256]{1,0:T(8,128)S(1)}, f32[32,256]{1,0:T(8,128)}, u32[]{:S(2)}) copy-start(f32[32,256]{1,0:T(8,128)} %get-tuple-element.28) | copy-start | bytes 98308
  86.5 0.8 copy-start.4

commit v2 on v1

--- a/solution.py
+++ b/solution.py
@@ -13,6 +13,8 @@
 scale_floor = 0.5
 learn_rate = 0.02
 MESH = pl.DeviceIdType.MESH
+VMEM_GRANT = 24 * 1024 * 1024
+SMALL_GRANT = 1024 * 1024
 ANY = pl.BlockSpec(memory_space=pl.ANY)
 
 
@@ -126,25 +128,27 @@
     gathered,
     mix,
     part,
-    landed,
+    near,
+    paired,
+    far,
     dirs,
     squares,
     update,
-    fresh,
-    copies,
     in_sem,
-    out_sem,
-    copy_sem,
     ring_a_send,
     ring_a_recv,
     ring_e_send,
     ring_e_recv,
     mix_send,
     mix_recv,
-    part_send,
-    part_recv,
+    near_send,
+    near_recv,
+    far_send,
+    far_recv,
     dir_send,
     dir_recv,
+    pass_send,
+    pass_recv,
     sq_send,
     sq_recv,
 ):
@@ -156,6 +160,15 @@
     rank_rows = first.shape[1]
     rank = n * rank_rows
     width = cot.shape[2]
+    planes = n // 2
+    side = me % 2
+    plane = me // 2
+    twin = me + 1 - 2 * side
+    copies = (cq_out, ck_out)
+    update_outs = (uq_out, uk_out)
+    new_outs = (nq_out, nk_out)
+    first_outs = (q1_out, k1_out)
+    second_outs = (q2_out, k2_out)
 
     loads = [
         pltpu.make_async_copy(src, dst, in_sem.at[i])
@@ -199,24 +212,17 @@
     ring.begin(1)
     loads[2].wait()
 
-    def product(owner, low, size, block):
-        columns = pl.ds(pl.multiple_of(owner * rows + low, 128), size)
-        mix[core] += jnp.dot(x[:, columns], block, preferred_element_type=jnp.float32)
-
-    mix[core] = jnp.dot(
-        x[:, pl.ds(pl.multiple_of(me * rows, 128), rows)],
-        fac[core],
-        preferred_element_type=jnp.float32,
-    )
-    for step in range(1, n // 2 + 1):
-        seen = []
-        ring.step(step, lambda owner, half: seen.append((owner, half)))
-        if step < n // 2:
-            for way in range(2):
-                owner = ring.owner(step, way)
-                product(owner, 0, rows, gathered[owner])
-        else:
-            product(ring.owner(step, 0), 0, rows, gathered[ring.owner(step, 0)])
+    def product(owner, block):
+        columns = pl.ds(pl.multiple_of(owner * rows, 128), rows)
+        return jnp.dot(x[:, columns], block, preferred_element_type=jnp.float32)
+
+    mixed = product(me, fac[core])
+    for step in range(1, planes + 1):
+        ring.step(step, lambda owner, half: None)
+        for way in range(2 if step < planes else 1):
+            owner = ring.owner(step, way)
+            mixed += product(owner, gathered[owner])
+    mix[core] = mixed
 
     swap = pltpu.make_async_remote_copy(
         src_ref=mix.at[core],
@@ -227,140 +233,152 @@
         device_id_type=MESH,
     )
     swap.start()
-    ring.finish()
     for load in loads[3:]:
         load.wait()
     swap.wait()
 
+    def to_near(p, k):
+        to = (plane + k) % planes
+        return pltpu.make_async_remote_copy(
+            src_ref=part.at[p, 2 * to + 1 - side],
+            dst_ref=near.at[p, to],
+            send_sem=near_send.at[p, k],
+            recv_sem=near_recv.at[p, k],
+            device_id={"fs": twin},
+            device_id_type=MESH,
+        )
+
+    def to_far(p, k):
+        to = (plane + k) % planes
+        return pltpu.make_async_remote_copy(
+            src_ref=paired.at[p, to],
+            dst_ref=far.at[p, plane],
+            send_sem=far_send.at[p, k],
+            recv_sem=far_recv.at[p, k],
+            device_id={"fs": 2 * to + side},
+            device_id_type=MESH,
+        )
+
+    order = tuple(range(1, planes)) + (0,)
     contract = (((0,), (0,)), ((), ()))
     for p in range(2):
         upper, lower = split_two(mix[p])
         total = lax.dot_general(upper, cot[p], contract, preferred_element_type=jnp.float32)
         total += lax.dot_general(lower, cot[p], contract, preferred_element_type=jnp.float32)
-        part[:, p] = total.reshape(n, rank_rows, width)
-
-    def share(k):
-        to = (me + k) % n
+        part[p] = total.reshape(n, rank_rows, width)
+        for k in order:
+            to_near(p, k).start()
+    for p in range(2):
+        for k in order:
+            to_near(p, k).wait_recv()
+            to = (plane + k) % planes
+            paired[p, to] = part[p, 2 * to + side] + near[p, to]
+            if k:
+                to_far(p, k).start()
+
+    def spread(p, k):
+        if k == 0:
+            to = twin
+        else:
+            to = 2 * ((plane + k) % planes) + side
         return pltpu.make_async_remote_copy(
-            src_ref=part.at[to],
-            dst_ref=landed.at[me],
-            send_sem=part_send.at[k - 1],
-            recv_sem=part_recv.at[k - 1],
+            src_ref=dirs.at[p, me],
+            dst_ref=dirs.at[p, me],
+            send_sem=dir_send.at[p, k],
+            recv_sem=dir_recv.at[p, k],
             device_id={"fs": to},
             device_id_type=MESH,
         )
 
-    for k in range(1, n):
-        share(k).start()
-    small = part[me]
-    for k in range(1, n):
-        share(k).wait_recv()
-        small += landed[(me - k + n) % n]
-
-    first_new, second_new, direction = moments(small, first[...], second[...])
-    dirs[me] = direction
-
-    def spread(k):
+    def hand_on(p, k):
+        owner = 2 * ((plane - k + planes) % planes) + side
         return pltpu.make_async_remote_copy(
-            src_ref=dirs.at[me],
-            dst_ref=dirs.at[me],
-            send_sem=dir_send.at[k - 1],
-            recv_sem=dir_recv.at[k - 1],
-            device_id={"fs": (me + k) % n},
+            src_ref=dirs.at[p, owner],
+            dst_ref=dirs.at[p, owner],
+            send_sem=pass_send.at[p, k - 1],
+            recv_sem=pass_recv.at[p, k - 1],
+            device_id={"fs": twin},
             device_id_type=MESH,
         )
 
-    for k in range(1, n):
-        spread(k).start()
-    first[...] = first_new
-    second[...] = second_new
-    outs = [
-        pltpu.make_async_copy(src, dst, out_sem.at[i])
-        for i, (src, dst) in enumerate(
-            (
-                (first.at[0], q1_out),
-                (first.at[1], k1_out),
-                (second.at[0], q2_out),
-                (second.at[1], k2_out),
-                (update.at[0], uq_out),
-                (update.at[1], uk_out),
-                (fresh.at[0], nq_out),
-                (fresh.at[1], nk_out),
-            )
-        )
-    ]
-    for out in outs[:4]:
-        out.start()
-    for k in range(1, n):
-        share(k).wait_send()
-    for k in range(1, n):
-        spread(k).wait_recv()
-
-    full = [dirs[:, p].reshape(rank, width) for p in range(2)]
-    for p in range(2):
-        squares[tp, p] = jnp.sum((full[p] * full[p]).reshape(rank // 8, 8, width), axis=0)
-
-    def tell(k):
+    def tell(p, k):
         return pltpu.make_async_remote_copy(
-            src_ref=squares.at[tp],
-            dst_ref=squares.at[tp],
-            send_sem=sq_send.at[k - 1],
-            recv_sem=sq_recv.at[k - 1],
+            src_ref=squares.at[p, tp],
+            dst_ref=squares.at[p, tp],
+            send_sem=sq_send.at[p, k - 1],
+            recv_sem=sq_recv.at[p, k - 1],
             device_id={"tp": (tp + k) % tps},
             device_id_type=MESH,
         )
 
-    for k in range(1, tps):
-        tell(k).start()
-    for p in range(2):
-        upper, lower = split_two(full[p])
+    for p in range(2):
+        small = paired[p, plane]
+        for k in range(1, planes):
+            to_far(p, k).wait_recv()
+            small += far[p, (plane - k + planes) % planes]
+        first_new, second_new, direction = moments(small, first[p], second[p])
+        dirs[p, me] = direction
+        for k in order:
+            spread(p, k).start()
+        first_outs[p][...] = first_new
+        second_outs[p][...] = second_new
+
+    for p in range(2):
+        for k in range(1, planes):
+            spread(p, k).wait_recv()
+            hand_on(p, k).start()
+    for p in range(2):
+        spread(p, 0).wait_recv()
+        for k in range(1, planes):
+            hand_on(p, k).wait_recv()
+        full = dirs[p].reshape(rank, width)
+        squares[p, tp] = jnp.sum((full * full).reshape(rank // 8, 8, width), axis=0)
+        for k in range(1, tps):
+            tell(p, k).start()
+        upper, lower = split_two(full)
         total = jnp.dot(fac[p], upper, preferred_element_type=jnp.float32)
         update[p] = total + jnp.dot(fac[p], lower, preferred_element_type=jnp.float32)
-    for k in range(1, tps):
-        tell(k).wait_recv()
-
-    ring = Ring(
-        n,
-        me,
-        lambda half: copies.at[me, half],
-        lambda owner, half: copies.at[owner, half],
-        ring_e_send,
-        ring_e_recv,
-    )
-    targets = (cq_out, ck_out)
-
-    def put(owner, half):
-        return pltpu.make_async_copy(
-            copies.at[owner, half],
-            targets[half].at[pl.ds(pl.multiple_of(owner * rows, 16), rows)],
-            copy_sem.at[owner, half],
-        )
-
-    for p in range(2):
-        square = jnp.sum(jnp.sum(squares[:, p], axis=0), keepdims=True)
+
+    def block(owner, half):
+        return copies[half].at[pl.ds(pl.multiple_of(owner * rows, 128), rows)]
+
+    outer = Ring(n, me, lambda half: block(me, half), block, ring_e_send, ring_e_recv)
+    for p in range(2):
+        for k in range(1, tps):
+            tell(p, k).wait_recv()
+        square = jnp.sum(jnp.sum(squares[p], axis=0), keepdims=True)
         scale = 1.0 / jnp.maximum(jnp.sqrt(square / (rank * width * tps)), scale_floor)
         step = -scale * update[p]
         made = weight[p] + learn_rate * step
-        copies[me, p] = made.astype(jnp.bfloat16)
-        ring.begin(p)
-        update[p] = step
-        fresh[p] = made
-        put(me, p).start()
-        outs[4 + p].start()
-        outs[6 + p].start()
-
-    for step in range(1, n // 2 + 1):
-        ring.step(step, lambda owner, half: put(owner, half).start())
-    for k in range(1, n):
-        spread(k).wait_send()
-    for k in range(1, tps):
-        tell(k).wait_send()
+        block(me, p)[...] = made.astype(jnp.bfloat16)
+        outer.begin(p)
+        update_outs[p][...] = step
+        new_outs[p][...] = made
+
+    for step in range(1, planes + 1):
+        outer.step(step, lambda owner, half: None)
     ring.finish()
-    for out in outs:
-        out.wait()
-    for owner in range(n):
-        for half in range(2):
-            put(owner, half).wait()
+    for p in range(2):
+        for k in order:
+            to_near(p, k).wait_send()
+            spread(p, k).wait_send()
+            if k:
+                to_far(p, k).wait_send()
+                hand_on(p, k).wait_send()
+        for k in range(1, tps):
+            tell(p, k).wait_send()
+    outer.finish()
+
+
+def settle(count, *refs):
+    sems = refs[2 * count]
+    moves = []
+    for i in range(count):
+        moves.append(pltpu.make_async_copy(refs[i], refs[count + i], sems.at[i]))
+    for move in moves:
+        move.start()
+    for move in moves:
+        move.wait()
 
 
 def fused_body(n, tps, *args):
@@ -369,49 +387,64 @@
     rows, rank = fac.shape
     width = cot.shape[1]
     rank_rows = first.shape[0]
+    planes = n // 2
     matrix = jax.ShapeDtypeStruct((rows, width), f32)
     copy = jax.ShapeDtypeStruct((rows * n, width), bf16)
     moment = jax.ShapeDtypeStruct((rank_rows, width), f32)
+    outs = (matrix, matrix, copy, moment, moment) * 2
     dma = pltpu.SemaphoreType.DMA
-    return pl.pallas_call(
+    vmem = pltpu.VMEM
+    made = pl.pallas_call(
         functools.partial(fused, n, tps),
-        out_shape=(matrix, matrix, copy, moment, moment) * 2,
-        in_specs=[ANY] * 11,
-        out_specs=(ANY,) * 10,
+        out_shape=outs,
+        in_specs=[pl.BlockSpec(memory_space=pltpu.HBM)] * 11,
+        out_specs=(pl.BlockSpec(memory_space=pltpu.VMEM),) * 10,
         scratch_shapes=[
-            pltpu.VMEM(x.shape, bf16),
-            pltpu.VMEM((2,) + cot.shape, bf16),
-            pltpu.VMEM((2,) + fac.shape, bf16),
-            pltpu.VMEM((2,) + first.shape, f32),
-            pltpu.VMEM((2,) + first.shape, f32),
-            pltpu.VMEM((2, rows, width), f32),
-            pltpu.VMEM((n,) + fac.shape, bf16),
-            pltpu.VMEM((2, x.shape[0], rank), f32),
-            pltpu.VMEM((n, 2) + first.shape, f32),
-            pltpu.VMEM((n, 2) + first.shape, f32),
-            pltpu.VMEM((n, 2) + first.shape, f32),
-            pltpu.VMEM((tps, 2, 8, width), f32),
-            pltpu.VMEM((2, rows, width), f32),
-            pltpu.VMEM((2, rows, width), f32),
-            pltpu.VMEM((n, 2, rows, width), bf16),
+            vmem(x.shape, bf16),
+            vmem((2,) + cot.shape, bf16),
+            vmem((2,) + fac.shape, bf16),
+            vmem((2,) + first.shape, f32),
+            vmem((2,) + first.shape, f32),
+            vmem((2, rows, width), f32),
+            vmem((n,) + fac.shape, bf16),
+            vmem((2, x.shape[0], rank), f32),
+            vmem((2, n) + first.shape, f32),
+            vmem((2, planes) + first.shape, f32),
+            vmem((2, planes) + first.shape, f32),
+            vmem((2, planes) + first.shape, f32),
+            vmem((2, n) + first.shape, f32),
+            vmem((2, tps, 8, width), f32),
+            vmem((2, rows, width), f32),
             dma((11,)),
-            dma((8,)),
-            dma((n, 2)),
-            dma((2, n // 2, 2)),
-            dma((2, n // 2, 2)),
-            dma((2, n // 2, 2)),
-            dma((2, n // 2, 2)),
+            dma((2, planes, 2)),
+            dma((2, planes, 2)),
+            dma((2, planes, 2)),
+            dma((2, planes, 2)),
             dma,
             dma,
-            dma((n - 1,)),
-            dma((n - 1,)),
-            dma((n - 1,)),
-            dma((n - 1,)),
-            dma((tps - 1,)),
-            dma((tps - 1,)),
+            dma((2, planes)),
+            dma((2, planes)),
+            dma((2, planes)),
+            dma((2, planes)),
+            dma((2, planes)),
+            dma((2, planes)),
+            dma((2, planes - 1)),
+            dma((2, planes - 1)),
+            dma((2, tps - 1)),
+            dma((2, tps - 1)),
         ],
-        compiler_params=pltpu.CompilerParams(collective_id=0, has_side_effects=True),
+        compiler_params=pltpu.CompilerParams(
+            collective_id=0, has_side_effects=True, vmem_limit_bytes=VMEM_GRANT
+        ),
     )(*args)
+    return pl.pallas_call(
+        functools.partial(settle, len(outs)),
+        out_shape=outs,
+        in_specs=[ANY] * len(outs),
+        out_specs=(ANY,) * len(outs),
+        scratch_shapes=[dma((len(outs),))],
+        compiler_params=pltpu.CompilerParams(vmem_limit_bytes=SMALL_GRANT),
+    )(*made)
 
 
 def split_three(values):

time: 88.1 us -> 82.6 us (0.938)
  Pallas kernels: 77.7 us -> 71.6 us
    pallas_call x1 -> x2, Pallas kernels: 77.7 us -> 71.6 us  [the longest x1 69.9 us: fused_body(): pl.pallas_call(functools.partial(fused, n, tps), out_shape=outs, in_specs...]
    unnamed x26 -> x22, local copies, waits for them, and re-layouts: 9.41 us -> 9.65 us
where the time goes in v2:
time: 82.6 us; the launch traced here: 82 us
  Pallas kernels  71.6 us (87%)
  local copies, waits for them, and re-layouts  9.65 us (12%)
    pallas_call x1, Pallas kernels, fused_body(): pl.pallas_call(functools.partial(fused, n, tps), out_shape=outs, in_specs...  69.9 us
    unnamed x22, local copies, waits for them, and re-layouts  9.65 us
    pallas_call x1, Pallas kernels, fused_body(): pl.pallas_call(functools.partial(settle, len(outs)), out_shape=outs, in_s...  1.78 us

profile of v2, /device:TPU:0, one launch (start us, length us, event | category | flops | bytes accessed | tf_op | source)
XLA Modules:
  0.0 82.0 jit_solution(11432190872700230273)
XLA Ops:
  0.6 0.0 copy-start
  0.7 1.1 %copy-done = bf16[192,2048]{1,0:T(8,128)(2,1)S(1)} copy-done((bf16[192,2048]{1,0:T(8,128)(2,1)S(1)}, bf16[192,2048]{1,0:T(8,128)(2,1)}, u32[]{:S(2)}) %copy-start) | copy-done | bytes 786456
  1.8 0.0 copy-start.1
  1.8 0.9 %copy-done.1 = f32[256,256]{1,0:T(8,128)S(1)} copy-done((f32[256,256]{1,0:T(8,128)S(1)}, f32[256,256]{1,0:T(8,128)}, u32[]{:S(2)}) %copy-start.1) | copy-done | bytes 262168
  2.7 0.0 copy-start.2
  2.7 0.9 %copy-done.2 = f32[256,256]{1,0:T(8,128)S(1)} copy-done((f32[256,256]{1,0:T(8,128)S(1)}, f32[256,256]{1,0:T(8,128)}, u32[]{:S(2)}) %copy-start.2) | copy-done | bytes 262168
  3.7 0.0 copy-start.3
  3.7 0.9 %copy-done.3 = bf16[256,256]{1,0:T(8,128)(2,1)S(1)} copy-done((bf16[256,256]{1,0:T(8,128)(2,1)S(1)}, bf16[256,256]{1,0:T(8,128)(2,1)}, u32[]{:S(2)}) %copy-start.3) | copy-done | bytes 131096
  4.6 0.0 copy-start.4
  4.6 0.9 %copy-done.4 = bf16[256,256]{1,0:T(8,128)(2,1)S(1)} copy-done((bf16[256,256]{1,0:T(8,128)(2,1)S(1)}, bf16[256,256]{1,0:T(8,128)(2,1)}, u32[]{:S(2)}) %copy-start.4) | copy-done | bytes 131096
  5.5 0.0 copy-start.5
  5.5 0.9 %copy-done.5 = bf16[192,256]{1,0:T(8,128)(2,1)S(1)} copy-done((bf16[192,256]{1,0:T(8,128)(2,1)S(1)}, bf16[192,256]{1,0:T(8,128)(2,1)}, u32[]{:S(2)}) %copy-start.5) | copy-done | bytes 98328
  6.4 0.0 copy-start.6
  6.4 0.9 %copy-done.6 = bf16[192,256]{1,0:T(8,128)(2,1)S(1)} copy-done((bf16[192,256]{1,0:T(8,128)(2,1)S(1)}, bf16[192,256]{1,0:T(8,128)(2,1)}, u32[]{:S(2)}) %copy-start.6) | copy-done | bytes 98328
  7.3 0.0 copy-start.7
  7.3 0.8 copy-done.7
  8.0 0.0 copy-start.8
  8.0 0.8 copy-done.8
  8.8 0.0 copy-start.9
  8.8 0.8 copy-done.9
  9.6 0.0 copy-start.10
  9.6 0.8 copy-done.10
  10.3 69.9 %shard_map.186 = (f32[256,256]{1,0:T(8,128)S(1)}, f32[256,256]{1,0:T(8,128)S(1)}, bf16[2048,256]{1,0:T(8,128)(2,1)S(1)}, f32[32,256]{1,0:T(8,128)S(1)}, f32[32,2...) custom-call(bf16[192,2048]{1,0:T(8,128)(2,1)S(1)} %copy-done, ...), custom_call_target="tpu_custom_call" | custom-call | tf_op jit(solution)/shard_map/pallas_call | solution.py:397
  80.2 1.8 %shard_map.187 = (f32[256,256]{1,0:T(8,128)}, f32[256,256]{1,0:T(8,128)}, bf16[2048,256]{1,0:T(8,128)(2,1)}, f32[32,256]{1,0:T(8,128)}, f32[32,256]{1,0:T(8,128)...) custom-call(f32[256,256]{1,0:T(8,128)S(1)} %get-tuple-element.20.ref, ...), custom_call_target="tpu_custom_call" | custom-call | tf_op jit(solution)/shard_map/pallas_call | solution.py:440
Async XLA Ops:
  0.6 1.1 %copy-start = (bf16[192,2048]{1,0:T(8,128)(2,1)S(1)}, bf16[192,2048]{1,0:T(8,128)(2,1)}, u32[]{:S(2)}) copy-start(bf16[192,2048]{1,0:T(8,128)(2,1)} %x_in.1) | copy-start | bytes 2359300
  1.8 0.9 %copy-start.1 = (f32[256,256]{1,0:T(8,128)S(1)}, f32[256,256]{1,0:T(8,128)}, u32[]{:S(2)}) copy-start(f32[256,256]{1,0:T(8,128)} %wq_in.1) | copy-start | bytes 786436
  2.7 0.9 %copy-start.2 = (f32[256,256]{1,0:T(8,128)S(1)}, f32[256,256]{1,0:T(8,128)}, u32[]{:S(2)}) copy-start(f32[256,256]{1,0:T(8,128)} %wk_in.1) | copy-start | bytes 786436
  3.7 0.9 %copy-start.3 = (bf16[256,256]{1,0:T(8,128)(2,1)S(1)}, bf16[256,256]{1,0:T(8,128)(2,1)}, u32[]{:S(2)}) copy-start(bf16[256,256]{1,0:T(8,128)(2,1)} %fq_in.1) | copy-start | bytes 393220
  4.6 0.9 %copy-start.4 = (bf16[256,256]{1,0:T(8,128)(2,1)S(1)}, bf16[256,256]{1,0:T(8,128)(2,1)}, u32[]{:S(2)}) copy-start(bf16[256,256]{1,0:T(8,128)(2,1)} %fk_in.1) | copy-start | bytes 393220
  5.5 0.9 %copy-start.5 = (bf16[192,256]{1,0:T(8,128)(2,1)S(1)}, bf16[192,256]{1,0:T(8,128)(2,1)}, u32[]{:S(2)}) copy-start(bf16[192,256]{1,0:T(8,128)(2,1)} %cq_in.1) | copy-start | bytes 294916
  6.4 0.9 %copy-start.6 = (bf16[192,256]{1,0:T(8,128)(2,1)S(1)}, bf16[192,256]{1,0:T(8,128)(2,1)}, u32[]{:S(2)}) copy-start(bf16[192,256]{1,0:T(8,128)(2,1)} %ck_in.1) | copy-start | bytes 294916
  7.3 0.8 copy-start.7
  8.0 0.8 copy-start.8
  8.8 0.8 copy-start.9
  9.6 0.8 copy-start.10

commit v3 on v2

--- a/solution.py
+++ b/solution.py
@@ -436,7 +436,7 @@
         compiler_params=pltpu.CompilerParams(
             collective_id=0, has_side_effects=True, vmem_limit_bytes=VMEM_GRANT
         ),
-    )(*args)
+    )(*[pltpu.with_memory_space_constraint(arg, pltpu.HBM) for arg in args])
     return pl.pallas_call(
         functools.partial(settle, len(outs)),
         out_shape=outs,

time: 82.6 us -> 71.8 us (0.87)
  local copies, waits for them, and re-layouts: 9.65 us -> 0 us
    unnamed x22 -> x0, local copies, waits for them, and re-layouts: 9.65 us -> none
where the time goes in v3:
time: 71.8 us; the launch traced here: 71.6 us
  Pallas kernels  71 us (99%)
    pallas_call x1, Pallas kernels, fused_body(): pl.pallas_call(functools.partial(fused, n, tps), out_shape=outs, in_specs...  69.2 us
    pallas_call x1, Pallas kernels, fused_body(): pl.pallas_call(functools.partial(settle, len(outs)), out_shape=outs, in_s...  1.78 us

profile of v3, /device:TPU:0, one launch (start us, length us, event | category | flops | bytes accessed | tf_op | source)
XLA Modules:
  0.0 71.6 jit_solution(2910614381033676014)
XLA Ops:
  0.6 69.2 %shard_map.186 = (f32[256,256]{1,0:T(8,128)S(1)}, f32[256,256]{1,0:T(8,128)S(1)}, bf16[2048,256]{1,0:T(8,128)(2,1)S(1)}, f32[32,256]{1,0:T(8,128)S(1)}, f32[32,2...) custom-call(bf16[192,2048]{1,0:T(8,128)(2,1)} %x_in.1, ...), custom_call_target="tpu_custom_call" | custom-call | tf_op jit(solution)/shard_map/pallas_call | solution.py:397
  69.9 1.8 %shard_map.187 = (f32[256,256]{1,0:T(8,128)}, f32[256,256]{1,0:T(8,128)}, bf16[2048,256]{1,0:T(8,128)(2,1)}, f32[32,256]{1,0:T(8,128)}, f32[32,256]{1,0:T(8,128)...) custom-call(f32[256,256]{1,0:T(8,128)S(1)} %get-tuple-element.20.ref, ...), custom_call_target="tpu_custom_call" | custom-call | tf_op jit(solution)/shard_map/pallas_call | solution.py:440

commit v4 on v3

--- a/solution.py
+++ b/solution.py
@@ -15,6 +15,8 @@
 MESH = pl.DeviceIdType.MESH
 VMEM_GRANT = 24 * 1024 * 1024
 SMALL_GRANT = 1024 * 1024
+A_PIECES = 4
+E_ROWS = 64
 ANY = pl.BlockSpec(memory_space=pl.ANY)
 
 
@@ -43,56 +45,56 @@
 
 
 class Ring:
-    def __init__(self, n, me, own, slot, send, recv):
-        self.n, self.own, self.slot, self.send, self.recv = n, own, slot, send, recv
-        self.me = me
+    def __init__(self, n, me, pieces, own, slot, send, recv):
+        self.n, self.me, self.pieces = n, me, pieces
+        self.own, self.slot, self.send, self.recv = own, slot, send, recv
         self.place = ring_place(me, n)
         self.last = n // 2
 
-    def active(self, step, way, half):
-        return step < self.last or (step == self.last and way == half)
+    def active(self, step, way, piece):
+        return step < self.last or (step == self.last and way == piece % 2)
 
     def owner(self, step, way):
         shift = -step if way == 0 else step
         return ring_index((self.place + shift + self.n) % self.n, self.n)
 
-    def copy(self, step, way, half):
+    def copy(self, step, way, piece):
         shift = 1 if way == 0 else self.n - 1
         to = ring_index((self.place + shift) % self.n, self.n)
         if step == 1:
-            owner, src = self.me, self.own(half)
+            owner, src = self.me, self.own(piece)
         else:
             owner = self.owner(step - 1, way)
-            src = self.slot(owner, half)
+            src = self.slot(owner, piece)
         return pltpu.make_async_remote_copy(
             src_ref=src,
-            dst_ref=self.slot(owner, half),
-            send_sem=self.send.at[way, step - 1, half],
-            recv_sem=self.recv.at[way, step - 1, half],
+            dst_ref=self.slot(owner, piece),
+            send_sem=self.send.at[way, step - 1, piece],
+            recv_sem=self.recv.at[way, step - 1, piece],
             device_id={"fs": to},
             device_id_type=MESH,
         )
 
-    def begin(self, half):
-        for way in range(2):
-            if self.active(1, way, half):
-                self.copy(1, way, half).start()
-
-    def step(self, step, arrived):
-        for half in range(2):
+    def begin(self, pieces):
+        for piece in pieces:
             for way in range(2):
-                if self.active(step, way, half):
-                    self.copy(step, way, half).wait_recv()
-                    if self.active(step + 1, way, half):
-                        self.copy(step + 1, way, half).start()
-                    arrived(self.owner(step, way), half)
+                if self.active(1, way, piece):
+                    self.copy(1, way, piece).start()
+
+    def step(self, step):
+        for piece in range(self.pieces):
+            for way in range(2):
+                if self.active(step, way, piece):
+                    self.copy(step, way, piece).wait_recv()
+                    if self.active(step + 1, way, piece):
+                        self.copy(step + 1, way, piece).start()
 
     def finish(self):
         for step in range(1, self.last + 1):
             for way in range(2):
-                for half in range(2):
-                    if self.active(step, way, half):
-                        self.copy(step, way, half).wait_send()
+                for piece in range(self.pieces):
+                    if self.active(step, way, piece):
+                        self.copy(step, way, piece).wait_send()
 
 
 def fused(
@@ -109,16 +111,11 @@
     k2_in,
     wq_in,
     wk_in,
-    uq_out,
-    nq_out,
-    cq_out,
-    q1_out,
-    q2_out,
-    uk_out,
-    nk_out,
-    ck_out,
-    k1_out,
-    k2_out,
+    update_out,
+    new_out,
+    copies,
+    first_out,
+    second_out,
     x,
     cot,
     fac,
@@ -133,7 +130,7 @@
     far,
     dirs,
     squares,
-    update,
+    sums,
     in_sem,
     ring_a_send,
     ring_a_recv,
@@ -155,8 +152,8 @@
     me = lax.axis_index("fs")
     tp = lax.axis_index("tp")
     core = tp % 2
+    chains = (0, 1)
     rows = fac.shape[1]
-    half_rows = rows // 2
     rank_rows = first.shape[1]
     rank = n * rank_rows
     width = cot.shape[2]
@@ -164,11 +161,6 @@
     side = me % 2
     plane = me // 2
     twin = me + 1 - 2 * side
-    copies = (cq_out, ck_out)
-    update_outs = (uq_out, uk_out)
-    new_outs = (nq_out, nk_out)
-    first_outs = (q1_out, k1_out)
-    second_outs = (q2_out, k2_out)
 
     loads = [
         pltpu.make_async_copy(src, dst, in_sem.at[i])
@@ -179,12 +171,12 @@
                 (x_in, x),
                 (cq_in, cot.at[0]),
                 (ck_in, cot.at[1]),
+                (wq_in, weight.at[0]),
+                (wk_in, weight.at[1]),
                 (q1_in, first.at[0]),
                 (k1_in, first.at[1]),
                 (q2_in, second.at[0]),
                 (k2_in, second.at[1]),
-                (wq_in, weight.at[0]),
-                (wk_in, weight.at[1]),
             )
         )
     ]
@@ -192,24 +184,27 @@
         load.start()
 
     barrier = pltpu.get_barrier_semaphore()
-    for k in range(1, n):
-        pl.semaphore_signal(barrier, inc=1, device_id={"fs": (me + k) % n}, device_id_type=MESH)
+    place = ring_place(me, n)
+    for shift in (1, n - 1):
+        to = ring_index((place + shift) % n, n)
+        pl.semaphore_signal(barrier, inc=1, device_id={"fs": to}, device_id_type=MESH)
     for k in range(1, tps):
         pl.semaphore_signal(barrier, inc=1, device_id={"tp": (tp + k) % tps}, device_id_type=MESH)
-    pl.semaphore_wait(barrier, n + tps - 2)
+    pl.semaphore_wait(barrier, 2 + tps - 1)
 
     loads[0].wait()
     loads[1].wait()
+    cut = rows // A_PIECES
     ring = Ring(
         n,
         me,
-        lambda half: fac.at[core, pl.ds(half * half_rows, half_rows)],
-        lambda owner, half: gathered.at[owner, pl.ds(half * half_rows, half_rows)],
+        A_PIECES,
+        lambda piece: fac.at[core, pl.ds(piece * cut, cut)],
+        lambda owner, piece: gathered.at[owner, pl.ds(piece * cut, cut)],
         ring_a_send,
         ring_a_recv,
     )
-    ring.begin(0)
-    ring.begin(1)
+    ring.begin(range(A_PIECES))
     loads[2].wait()
 
     def product(owner, block):
@@ -217,12 +212,16 @@
         return jnp.dot(x[:, columns], block, preferred_element_type=jnp.float32)
 
     mixed = product(me, fac[core])
-    for step in range(1, planes + 1):
-        ring.step(step, lambda owner, half: None)
-        for way in range(2 if step < planes else 1):
+    for step in range(1, planes):
+        ring.step(step)
+        for way in range(2):
             owner = ring.owner(step, way)
             mixed += product(owner, gathered[owner])
-    mix[core] = mixed
+    loads[5].wait()
+    loads[6].wait()
+    ring.step(planes)
+    owner = ring.owner(planes, 0)
+    mix[core] = mixed + product(owner, gathered[owner])
 
     swap = pltpu.make_async_remote_copy(
         src_ref=mix.at[core],
@@ -233,26 +232,25 @@
         device_id_type=MESH,
     )
     swap.start()
-    for load in loads[3:]:
-        load.wait()
-    swap.wait()
-
-    def to_near(p, k):
+    loads[3].wait()
+    loads[4].wait()
+
+    def to_near(p, c, k):
         to = (plane + k) % planes
         return pltpu.make_async_remote_copy(
-            src_ref=part.at[p, 2 * to + 1 - side],
-            dst_ref=near.at[p, to],
+            src_ref=part.at[c, 2 * to + 1 - side],
+            dst_ref=near.at[c, to],
             send_sem=near_send.at[p, k],
             recv_sem=near_recv.at[p, k],
             device_id={"fs": twin},
             device_id_type=MESH,
         )
 
-    def to_far(p, k):
+    def to_far(p, c, k):
         to = (plane + k) % planes
         return pltpu.make_async_remote_copy(
-            src_ref=paired.at[p, to],
-            dst_ref=far.at[p, plane],
+            src_ref=paired.at[c, to],
+            dst_ref=far.at[c, plane],
             send_sem=far_send.at[p, k],
             recv_sem=far_recv.at[p, k],
             device_id={"fs": 2 * to + side},
@@ -261,29 +259,33 @@
 
     order = tuple(range(1, planes)) + (0,)
     contract = (((0,), (0,)), ((), ()))
-    for p in range(2):
-        upper, lower = split_two(mix[p])
-        total = lax.dot_general(upper, cot[p], contract, preferred_element_type=jnp.float32)
-        total += lax.dot_general(lower, cot[p], contract, preferred_element_type=jnp.float32)
-        part[p] = total.reshape(n, rank_rows, width)
+    for p, c in enumerate(chains):
+        if p == 0:
+            swap.wait()
+        upper, lower = split_two(mix[c])
+        total = lax.dot_general(upper, cot[c], contract, preferred_element_type=jnp.float32)
+        total += lax.dot_general(lower, cot[c], contract, preferred_element_type=jnp.float32)
+        part[c] = total.reshape(n, rank_rows, width)
         for k in order:
-            to_near(p, k).start()
-    for p in range(2):
+            to_near(p, c, k).start()
+    for load in loads[7:]:
+        load.wait()
+    for p, c in enumerate(chains):
         for k in order:
-            to_near(p, k).wait_recv()
+            to_near(p, c, k).wait_recv()
             to = (plane + k) % planes
-            paired[p, to] = part[p, 2 * to + side] + near[p, to]
+            paired[c, to] = part[c, 2 * to + side] + near[c, to]
             if k:
-                to_far(p, k).start()
+                to_far(p, c, k).start()
+
+    def held(p, owner):
+        return sums.at[p - 2, owner] if p >= 2 else dirs.at[p, owner]
 
     def spread(p, k):
-        if k == 0:
-            to = twin
-        else:
-            to = 2 * ((plane + k) % planes) + side
+        to = 2 * ((plane + k) % planes) + side if k else twin
         return pltpu.make_async_remote_copy(
-            src_ref=dirs.at[p, me],
-            dst_ref=dirs.at[p, me],
+            src_ref=held(p, me),
+            dst_ref=held(p, me),
             send_sem=dir_send.at[p, k],
             recv_sem=dir_recv.at[p, k],
             device_id={"fs": to},
@@ -293,8 +295,8 @@
     def hand_on(p, k):
         owner = 2 * ((plane - k + planes) % planes) + side
         return pltpu.make_async_remote_copy(
-            src_ref=dirs.at[p, owner],
-            dst_ref=dirs.at[p, owner],
+            src_ref=held(p, owner),
+            dst_ref=held(p, owner),
             send_sem=pass_send.at[p, k - 1],
             recv_sem=pass_recv.at[p, k - 1],
             device_id={"fs": twin},
@@ -311,70 +313,100 @@
             device_id_type=MESH,
         )
 
-    for p in range(2):
+    def move(p):
         small = paired[p, plane]
         for k in range(1, planes):
-            to_far(p, k).wait_recv()
+            to_far(p, p, k).wait_recv()
             small += far[p, (plane - k + planes) % planes]
         first_new, second_new, direction = moments(small, first[p], second[p])
         dirs[p, me] = direction
+        squared = jnp.sum((direction * direction).reshape(rank_rows // 8, 8, width), axis=0)
+        squares[p, tp] = sum(squared[:, low : low + 128] for low in range(0, width, 128))
+        for k in range(1, tps):
+            tell(p, k).start()
+        first_out[p] = first_new
+        second_out[p] = second_new
+
+    def send(p):
         for k in order:
             spread(p, k).start()
-        first_outs[p][...] = first_new
-        second_outs[p][...] = second_new
-
-    for p in range(2):
+
+    def add_squares(p):
+        for k in range(1, tps):
+            tell(p, k).wait_recv()
+        sums[p, me] = jnp.sum(squares[p], axis=0)
+        send(2 + p)
+
+    def relay(p):
         for k in range(1, planes):
             spread(p, k).wait_recv()
             hand_on(p, k).start()
-    for p in range(2):
-        spread(p, 0).wait_recv()
-        for k in range(1, planes):
-            hand_on(p, k).wait_recv()
-        full = dirs[p].reshape(rank, width)
-        squares[p, tp] = jnp.sum((full * full).reshape(rank // 8, 8, width), axis=0)
-        for k in range(1, tps):
-            tell(p, k).start()
-        upper, lower = split_two(full)
-        total = jnp.dot(fac[p], upper, preferred_element_type=jnp.float32)
-        update[p] = total + jnp.dot(fac[p], lower, preferred_element_type=jnp.float32)
-
-    def block(owner, half):
-        return copies[half].at[pl.ds(pl.multiple_of(owner * rows, 128), rows)]
-
-    outer = Ring(n, me, lambda half: block(me, half), block, ring_e_send, ring_e_recv)
-    for p in range(2):
-        for k in range(1, tps):
-            tell(p, k).wait_recv()
-        square = jnp.sum(jnp.sum(squares[p], axis=0), keepdims=True)
+
+    def block(c, owner, low, size):
+        return copies.at[c, pl.ds(pl.multiple_of(owner * rows + low, 16), size)]
+
+    slabs = [(p, low) for p in range(2) for low in range(0, rows, E_ROWS)]
+
+    def slab(owner, piece):
+        p, low = slabs[piece]
+        return block(p, owner, low, E_ROWS)
+
+    outer = Ring(n, me, len(slabs), lambda piece: slab(me, piece), slab, ring_e_send, ring_e_recv)
+
+    def renew(p):
+        for q in (p, 2 + p):
+            spread(q, 0).wait_recv()
+            for k in range(1, planes):
+                hand_on(q, k).wait_recv()
+        square = jnp.sum(jnp.sum(sums[p], axis=0), keepdims=True)
         scale = 1.0 / jnp.maximum(jnp.sqrt(square / (rank * width * tps)), scale_floor)
-        step = -scale * update[p]
+        upper, lower = split_two(dirs[p].reshape(rank, width))
+        made = jnp.dot(fac[p], upper, preferred_element_type=jnp.float32)
+        made += jnp.dot(fac[p], lower, preferred_element_type=jnp.float32)
+        step = -scale * made
         made = weight[p] + learn_rate * step
-        block(me, p)[...] = made.astype(jnp.bfloat16)
-        outer.begin(p)
-        update_outs[p][...] = step
-        new_outs[p][...] = made
-
+        block(p, me, 0, rows)[...] = made.astype(jnp.bfloat16)
+        outer.begin([i for i in range(len(slabs)) if slabs[i][0] == p])
+        update_out[p] = step
+        new_out[p] = made
+
+    move(0)
+    send(0)
+    move(1)
+    add_squares(0)
+    send(1)
+    relay(0)
+    relay(2)
+    add_squares(1)
+    renew(0)
+    relay(1)
+    relay(3)
+    renew(1)
     for step in range(1, planes + 1):
-        outer.step(step, lambda owner, half: None)
+        outer.step(step)
     ring.finish()
-    for p in range(2):
+    for p, c in enumerate(chains):
         for k in order:
-            to_near(p, k).wait_send()
+            to_near(p, c, k).wait_send()
+            if k:
+                to_far(p, c, k).wait_send()
+    for p in range(4):
+        for k in order:
             spread(p, k).wait_send()
             if k:
-                to_far(p, k).wait_send()
                 hand_on(p, k).wait_send()
+    for p in range(2):
         for k in range(1, tps):
             tell(p, k).wait_send()
     outer.finish()
 
 
 def settle(count, *refs):
-    sems = refs[2 * count]
+    sems = refs[3 * count]
     moves = []
     for i in range(count):
-        moves.append(pltpu.make_async_copy(refs[i], refs[count + i], sems.at[i]))
+        for p in range(2):
+            moves.append(pltpu.make_async_copy(refs[i].at[p], refs[(1 + p) * count + i], sems.at[p, i]))
     for move in moves:
         move.start()
     for move in moves:
@@ -391,14 +423,15 @@
     matrix = jax.ShapeDtypeStruct((rows, width), f32)
     copy = jax.ShapeDtypeStruct((rows * n, width), bf16)
     moment = jax.ShapeDtypeStruct((rank_rows, width), f32)
-    outs = (matrix, matrix, copy, moment, moment) * 2
+    outs = (matrix, matrix, copy, moment, moment)
+    e_pieces = 2 * rows // E_ROWS
     dma = pltpu.SemaphoreType.DMA
     vmem = pltpu.VMEM
     made = pl.pallas_call(
         functools.partial(fused, n, tps),
-        out_shape=outs,
+        out_shape=tuple(jax.ShapeDtypeStruct((2,) + out.shape, out.dtype) for out in outs),
         in_specs=[pl.BlockSpec(memory_space=pltpu.HBM)] * 11,
-        out_specs=(pl.BlockSpec(memory_space=pltpu.VMEM),) * 10,
+        out_specs=(pl.BlockSpec(memory_space=pltpu.VMEM),) * 5,
         scratch_shapes=[
             vmem(x.shape, bf16),
             vmem((2,) + cot.shape, bf16),
@@ -413,23 +446,23 @@
             vmem((2, planes) + first.shape, f32),
             vmem((2, planes) + first.shape, f32),
             vmem((2, n) + first.shape, f32),
-            vmem((2, tps, 8, width), f32),
-            vmem((2, rows, width), f32),
+            vmem((2, tps, 8, 128), f32),
+            vmem((2, n, 8, 128), f32),
             dma((11,)),
-            dma((2, planes, 2)),
-            dma((2, planes, 2)),
-            dma((2, planes, 2)),
-            dma((2, planes, 2)),
+            dma((2, planes, A_PIECES)),
+            dma((2, planes, A_PIECES)),
+            dma((2, planes, e_pieces)),
+            dma((2, planes, e_pieces)),
             dma,
             dma,
             dma((2, planes)),
             dma((2, planes)),
             dma((2, planes)),
             dma((2, planes)),
-            dma((2, planes)),
-            dma((2, planes)),
-            dma((2, planes - 1)),
-            dma((2, planes - 1)),
+            dma((4, planes)),
+            dma((4, planes)),
+            dma((4, planes - 1)),
+            dma((4, planes - 1)),
             dma((2, tps - 1)),
             dma((2, tps - 1)),
         ],
@@ -437,14 +470,15 @@
             collective_id=0, has_side_effects=True, vmem_limit_bytes=VMEM_GRANT
         ),
     )(*[pltpu.with_memory_space_constraint(arg, pltpu.HBM) for arg in args])
-    return pl.pallas_call(
+    done = pl.pallas_call(
         functools.partial(settle, len(outs)),
-        out_shape=outs,
+        out_shape=outs * 2,
         in_specs=[ANY] * len(outs),
-        out_specs=(ANY,) * len(outs),
-        scratch_shapes=[dma((len(outs),))],
+        out_specs=(ANY,) * (2 * len(outs)),
+        scratch_shapes=[dma((2, len(outs)))],
         compiler_params=pltpu.CompilerParams(vmem_limit_bytes=SMALL_GRANT),
     )(*made)
+    return tuple(done)
 
 
 def split_three(values):

time: 71.8 us -> 69.2 us (0.964)
  Pallas kernels: 71 us -> 68.3 us
    pallas_call x2, Pallas kernels: 71 us -> 68.3 us  [the longest x1 66.6 us: fused_body(): pl.pallas_call(functools.partial(fused, n, tps), out_shape=tuple((jax.Sha...]
where the time goes in v4:
time: 69.2 us; the launch traced here: 69 us
  Pallas kernels  68.3 us (99%)
    pallas_call x1, Pallas kernels, fused_body(): pl.pallas_call(functools.partial(fused, n, tps), out_shape=tuple((jax.Sha...  66.6 us
    pallas_call x1, Pallas kernels, fused_body(): pl.pallas_call(functools.partial(settle, len(outs)), out_shape=outs * 2,...  1.77 us

profile of v4, /device:TPU:0, one launch (start us, length us, event | category | flops | bytes accessed | tf_op | source)
XLA Modules:
  0.0 69.0 jit_solution(3002368819064740406)
XLA Ops:
  0.6 66.6 %shard_map.186 = (f32[2,256,256]{2,1,0:T(8,128)S(1)}, f32[2,256,256]{2,1,0:T(8,128)S(1)}, bf16[2,2048,256]{2,1,0:T(8,128)(2,1)S(1)}, f32[2,32,256]{2,1,0:T(8,128)S(1)}, f32[2,32,256]{2,1,0:T(8,128)S(1)}) custom-call(bf16[192,2048]{1,0:T(8,128)(2,1)} %x_in.1, bf16[192,256]{1,0:T(8,128)(2,1)} %cq_in.1, bf16[192,256]{1,0:T(8,128)(2,1)} %ck_in.1, ...), custom_call_target="tpu_custom_call" | custom-call | tf_op jit(solution)/shard_map/pallas_call | solution.py:430
  67.2 1.8 %shard_map.187 = (f32[256,256]{1,0:T(8,128)}, f32[256,256]{1,0:T(8,128)}, bf16[2048,256]{1,0:T(8,128)(2,1)}, f32[32,256]{1,0:T(8,128)}, f32[32,256]{1,0:T(8,128)...) custom-call(f32[2,256,256]{2,1,0:T(8,128)S(1)} %get-tuple-element.15, ...), custom_call_target="tpu_custom_call" | custom-call | tf_op jit(solution)/shard_map/pallas_call | solution.py:473

commit v5 on v4

--- a/solution.py
+++ b/solution.py
@@ -378,8 +378,8 @@
     relay(0)
     relay(2)
     add_squares(1)
+    relay(1)
     renew(0)
-    relay(1)
     relay(3)
     renew(1)
     for step in range(1, planes + 1):

time: 69.2 us -> 68 us (0.983)
  Pallas kernels: 68.3 us -> 67.2 us
    pallas_call x1, Pallas kernels: 66.6 us -> 65.4 us  [fused_body(): pl.pallas_call(functools.partial(fused, n, tps), out_shape=tuple((jax.Sha...]
where the time goes in v5:
time: 68 us; the launch traced here: 67.9 us
  Pallas kernels  67.2 us (99%)
    pallas_call x1, Pallas kernels, fused_body(): pl.pallas_call(functools.partial(fused, n, tps), out_shape=tuple((jax.Sha...  65.4 us
    pallas_call x1, Pallas kernels, fused_body(): pl.pallas_call(functools.partial(settle, len(outs)), out_shape=outs * 2,...  1.77 us

profile of v5, /device:TPU:0, one launch (start us, length us, event | category | flops | bytes accessed | tf_op | source)
XLA Modules:
  0.0 67.9 jit_solution(3369499494940201688)
XLA Ops:
  0.6 65.4 %shard_map.186 = (f32[2,256,256]{2,1,0:T(8,128)S(1)}, f32[2,256,256]{2,1,0:T(8,128)S(1)}, bf16[2,2048,256]{2,1,0:T(8,128)(2,1)S(1)}, f32[2,32,256]{2,1,0:T(8,128)S(1)}, f32[2,32,256]{2,1,0:T(8,128)S(1)}) custom-call(bf16[192,2048]{1,0:T(8,128)(2,1)} %x_in.1, bf16[192,256]{1,0:T(8,128)(2,1)} %cq_in.1, bf16[192,256]{1,0:T(8,128)(2,1)} %ck_in.1, ...), custom_call_target="tpu_custom_call" | custom-call | tf_op jit(solution)/shard_map/pallas_call | solution.py:430
  66.1 1.8 %shard_map.187 = (f32[256,256]{1,0:T(8,128)}, f32[256,256]{1,0:T(8,128)}, bf16[2048,256]{1,0:T(8,128)(2,1)}, f32[32,256]{1,0:T(8,128)}, f32[32,256]{1,0:T(8,128)...) custom-call(f32[2,256,256]{2,1,0:T(8,128)S(1)} %get-tuple-element.15, ...), custom_call_target="tpu_custom_call" | custom-call | tf_op jit(solution)/shard_map/pallas_call | solution.py:473
